TPU v7x, 32 devices: a whole 2x2x4 slice. The times are simulated.
32 devices in a mesh: sp: 16 (over z, y, core), tp: 2 (over x).
Axes of the slice: x: 2, y: 2, z: 4, core: 2. Of those that a mesh axis runs over, the one named last changes fastest.
Arguments:
- tokens: bfloat16 [1, 8192, 2048], P(None, ('sp', 'tp')), may hold values from -6 to 6
- input_norm_gain: float32 [2048], replicated, may hold values from 0.1 to 1.9
- query_weight: bfloat16 [2048, 1024], P(None, 'tp'), may hold values from -0.125 to 0.125
- forget_weight: bfloat16 [2048, 1024], P(None, 'tp'), may hold values from -0.125 to 0.125
- input_weight: bfloat16 [2048, 1024], P(None, 'tp'), may hold values from -0.125 to 0.125
- gate_weight: bfloat16 [2048, 1024], P(None, 'tp'), may hold values from -0.125 to 0.125
- slack: float32 [1024], P('tp'), may hold values from 0 to 0.06
- sudden_decay: float32 [1, 8192, 8], P(None, 'sp', 'tp'), may hold values from -0.75 to 0
- head_norm_gain: float32 [128], replicated, may hold values from 0.1 to 1.9
- output_weight: bfloat16 [1024, 2048], P(None, 'tp'), may hold values from -1.25 to 1.25
- output_norm_gain: float32 [2048], P('tp'), may hold values from 0.1 to 1.9
Outputs:
- mixer_output: bfloat16 [1, 8192, 2048], P(None, 'sp', 'tp')
All inputs are finite; a program needn't handle non-finite values.
Results may differ from a plain program's by a relative error of at most 0.0094.
Values may be sent and summed in bfloat16 or wider, within the bound.
A program may use at most 64 MiB of HBM per device.

v0:
```python
import jax
import jax.numpy as jnp
from jax import lax
from jax.sharding import PartitionSpec as P

D = 2048
KEY = 128
BLOCK = 64


epsilon = 1e-06
precise = lax.Precision.HIGHEST


def entering(part, axis, combine, identity):
    place = lax.axis_index(axis)
    gathered = jax.tree.map(lambda a: lax.all_gather(a, axis), part)
    state = jax.tree.map(lambda a, e: jnp.zeros_like(a) + jnp.asarray(e, a.dtype), part, identity)

    def one(turn, state):
        return combine(
            state, jax.tree.map(lambda a: lax.dynamic_index_in_dim(a, turn, 0, False), gathered)
        )

    return lax.fori_loop(0, place, one, state)


def normalize(tensor_in, gain_vec):
    tensor_in = tensor_in.astype(jnp.float32)
    return (
        tensor_in
        * lax.rsqrt(jnp.mean(tensor_in * tensor_in, axis=-1, keepdims=True) + epsilon)
        * gain_vec
    )


def setup_params(query_logits, forget_logits, input_logits, slack, sudden_decay):
    sequence_total, sequence_span, local_heads = sudden_decay.shape

    def heads_first(tensor):
        return (
            tensor.astype(jnp.float32)
            .reshape(sequence_total, sequence_span, local_heads, -1)
            .transpose(0, 2, 1, 3)
        )

    query_rows = heads_first(query_logits) * KEY ** (-0.5)
    incoming_weights = slack.reshape(local_heads, -1)[None, :, None, :] * jax.nn.sigmoid(
        -heads_first(forget_logits)
    )
    forget_logarithm = jnp.log1p(-incoming_weights) + sudden_decay.transpose(0, 2, 1)[:, :, :, None]
    return (query_rows, incoming_weights, heads_first(input_logits), forget_logarithm)


def block_pass(query_rows, incoming_weights, value_rows, forget_logarithm, initial):
    sequence_total, local_heads, sequence_span, key_width = query_rows.shape
    blocks_here = sequence_span // BLOCK

    def by_block(tensor):
        return tensor.reshape(
            sequence_total, local_heads, blocks_here, BLOCK, tensor.shape[3]
        ).transpose(2, 0, 1, 3, 4)

    causal = jnp.tril(jnp.ones((BLOCK, BLOCK), dtype=bool))

    def advance(carried, portions):
        query_blk, weight_blk, value_blk, forget_blk = portions
        running = jnp.cumsum(forget_blk, axis=2)
        lifted_q = query_blk * jnp.exp(running)
        lifted_k = weight_blk * jnp.exp(-running)
        scores = jnp.einsum("shtk,shuk->shtu", lifted_q, lifted_k, precision=precise)
        scores = jnp.where(causal, scores, 0.0)
        produced = jnp.einsum("shtu,shuv->shtv", scores, value_blk, precision=precise) + jnp.einsum(
            "shtk,shkv->shtv", lifted_q, carried, precision=precise
        )
        ending = running[:, :, -1:, :]
        carried = jnp.exp(ending[:, :, 0, :])[..., None] * carried + jnp.einsum(
            "shuk,shuv->shkv", weight_blk * jnp.exp(ending - running), value_blk, precision=precise
        )
        return (carried, produced)

    final_state, produced = lax.scan(
        advance,
        initial,
        (
            by_block(query_rows),
            by_block(incoming_weights),
            by_block(value_rows),
            by_block(forget_logarithm),
        ),
    )
    return (
        final_state,
        produced.transpose(1, 2, 0, 3, 4).reshape(
            sequence_total, local_heads, sequence_span, value_rows.shape[3]
        ),
    )


def gate_heads(produced, gate_raw, head_norm_gain):
    sequence_total, local_heads, sequence_span, val_width = produced.shape
    mean_sq = jnp.mean(produced * produced, axis=3, keepdims=True)
    scaled = produced * lax.rsqrt(mean_sq + epsilon) * head_norm_gain
    scaled = scaled.transpose(0, 2, 1, 3).reshape(
        sequence_total, sequence_span, local_heads * val_width
    )
    return (scaled * jax.nn.silu(gate_raw.astype(jnp.float32))).astype(jnp.bfloat16)


def join_states(earlier, later):
    earlier_decay, earlier_state = earlier
    later_decay, later_state = later
    return (
        earlier_decay + later_decay,
        jnp.exp(later_decay)[..., None] * earlier_state + later_state,
    )


def recurrence(query_rows, incoming_weights, value_rows, forget_logarithm):
    sequence_total, local_heads, sequence_span, key_width = query_rows.shape
    val_width = value_rows.shape[3]
    through = jnp.cumsum(forget_logarithm, axis=2)
    totals = through[:, :, -1, :]
    head_spans = (0, local_heads)
    head_from, head_upto = head_spans
    zero_state = jnp.zeros(
        (sequence_total, head_upto - head_from, key_width, val_width), jnp.float32
    )
    final_state, produced = block_pass(
        query_rows, incoming_weights, value_rows, forget_logarithm, zero_state
    )
    identity = (jnp.zeros_like(totals), jnp.zeros_like(final_state))
    incoming = entering((totals, final_state), "sp", join_states, identity)
    incoming = incoming[1]
    readout = jnp.einsum(
        "shtk,shkv->shtv", query_rows * jnp.exp(through), incoming, precision=precise
    )
    outputs = produced + readout
    return outputs


def shards(
    tokens,
    input_norm_gain,
    query_weight,
    forget_weight,
    input_weight,
    gate_weight,
    slack,
    sudden_decay,
    head_norm_gain,
    output_weight,
    output_norm_gain,
):
    normed = normalize(tokens, input_norm_gain).astype(jnp.bfloat16)
    matrices = (query_weight, forget_weight, input_weight, gate_weight)
    portion = lax.all_gather(normed, "tp", axis=1, tiled=True)
    joined = lax.optimization_barrier(
        jnp.concatenate(
            [
                jnp.einsum(
                    "std,dc->stc", portion, matrix, preferred_element_type=jnp.float32
                ).astype(jnp.bfloat16)
                for matrix in matrices
            ],
            axis=2,
        )
    )
    query_cols = query_weight.shape[1]
    input_cols = input_weight.shape[1]
    query_logits = joined[:, :, :query_cols]
    forget_logits = joined[:, :, query_cols : 2 * query_cols]
    input_logits = joined[:, :, 2 * query_cols : 2 * query_cols + input_cols]
    gate_raw = joined[:, :, 2 * query_cols + input_cols :]
    query_rows, incoming_weights, value_rows, forget_logarithm = setup_params(
        query_logits, forget_logits, input_logits, slack, sudden_decay
    )
    produced = recurrence(query_rows, incoming_weights, value_rows, forget_logarithm)
    gated_out = gate_heads(produced, gate_raw, head_norm_gain)
    projected = jnp.einsum(
        "stc,cd->std",
        lax.all_gather(gated_out, "tp", axis=2, tiled=True),
        output_weight,
        preferred_element_type=jnp.float32,
    )
    squares = lax.psum(jnp.sum(projected * projected, axis=2, keepdims=True), "tp")
    return (projected * lax.rsqrt(squares / D + epsilon) * output_norm_gain).astype(jnp.bfloat16)


def solution(mesh):
    placed = (
        P(None, ("sp", "tp"), None),
        P(),
        P(None, "tp"),
        P(None, "tp"),
        P(None, "tp"),
        P(None, "tp"),
        P("tp"),
        P(None, "sp", "tp"),
        P(),
        P(None, "tp"),
        P("tp"),
    )
    return jax.shard_map(
        shards, mesh=mesh, in_specs=placed, out_specs=P(None, "sp", "tp"), check_vma=False
    )
```

profile of v0, /device:TPU:28, one launch (start us, length us, event | category | flops | bytes accessed | tf_op | source)
XLA Modules:
  0.0 235.8 jit_solution(12733148455241337241)
XLA Ops:
  8.2 2.5 %fusion.28 = bf16[1,256,2048]{2,1,0:T(8,128)(2,1)} fusion(bf16[1,256,2048]{2,1,0:T(8,128)(2,1)} %param.15, f32[2048]{0:T(1024)} %param.16, f32[256]{0:T(256)S(1)} %add_rsqrt_fusion.2), kind=kLoop, calls=%fused_computation.40 | loop fusion | flops 2097152 | bytes 2106368 | tf_op jit(solution)/shard_map/convert_element_type | solution.py:155
  10.8 34.1 %all-gather.6.cloned.1.call-done = bf16[1,512,2048]{2,1,0:T(8,128)(2,1)} async-done(((bf16[1,256,2048]{2,1,0:T(8,128)(2,1)}), bf16[1,512,2048]{2,1,0:T(8,128)(2,1)}) %all-gather.6.cloned.1.call-update) | async-done | bytes 2097168 | tf_op jit(solution)/shard_map/all_gather | solution.py:157
  44.9 3.7 %fusion.49 = bf16[1,512,512]{1,2,0:T(8,128)(2,1)S(1)} fusion(bf16[2048,512]{1,0:T(8,128)(2,1)} %param.20, bf16[1,512,2048]{2,1,0:T(8,128)(2,1)} %all-gather.6.cloned.1.call-done), kind=kOutput, calls=%fused_computation.59 | convolution fusion | flops 1074003968 | bytes 4718592 | tf_op jit(solution)/shard_map/std,dc->stc/dot_general | solution.py:161
  56.2 3.1 %bitcast_add_fusion.2 = (f32[1,4,128,512]{2,3,1,0:T(8,128)}, f32[1,512,4,128]{3,1,2,0:T(8,128)}) fusion(f32[4,512]{1,0:T(4,128)S(1)} %bitcast.243, f32[1,512,4,128]{3,1,2,0:T(8,128)} %copy.32, f32[4,128]{1,0:T(4,128)S(1)} %bitcast.248), kind=kLoop, calls=%fused_computation.72 | loop fusion | flops 786432 | bytes 3155968 | tf_op jit(solution)/shard_map/add | solution.py:51
  59.3 2.6 %fusion.70 = f32[1,4,512,128]{3,2,1,0:T(8,128)} fusion(f32[1,512,4,128]{3,1,2,0:T(8,128)} %get-tuple-element.175, f32[4,512]{1,0:T(4,128)S(1)} %bitcast.244), kind=kLoop, calls=%fused_computation.76 | loop fusion | flops 524288 | bytes 2105344 | tf_op jit(solution)/shard_map/add | solution.py:51
  63.1 2.6 %copy.34 = f32[1,512,4,128]{3,1,2,0:T(8,128)} copy(f32[1,512,4,128]{1,3,2,0:T(8,128)} %bitcast.233) | data formatting | bytes 2097152 | tf_op jit(solution)/shard_map/mul | solution.py:47
  65.7 57.5 %while.26 = (s32[]{:T(128)}, f32[1,4,128,128]{3,2,1,0:T(8,128)S(1)}, f32[8,1,4,64,128]{4,3,0,2,1:T(8,128)}, f32[8,1,4,64,128]{4,3,0,2,1:T(8,128)}, f32[8,1,4,64,...) while((s32[]{:T(128)}, ...), condition=%wide.region_3.4_spmd.clone, body=%wide.region_1.3_spmd.clone.sunk | while | flops 153571328 | bytes 3174530 | solution.py:82
  69.2 1.9 fusion.96
  76.4 1.9 fusion.96
  83.6 1.9 fusion.96
  90.8 1.9 fusion.96
  98.0 1.9 fusion.96
  105.2 1.9 fusion.96
  112.4 1.9 fusion.96
  119.6 1.9 fusion.96
  124.0 2.5 %copy.46 = f32[4,512,128]{1,2,0:T(8,128)} copy(f32[4,512,128]{2,1,0:T(8,128)} %bitcast.238) | data formatting | bytes 2097152 | tf_op jit(solution)/shard_map/reshape | solution.py:94
  128.5 16.8 %all-gather = f32[16,4,1,128]{3,1,2,0:T(4,128)S(1)} all-gather(f32[1,4,1,128]{3,1,2,0:T(4,128)S(1)} %bitcast.246), channel_id=2, replica_groups=mesh['sp'=16,'tp'=2] {'sp'}, dimensions={0}, use_global_device_ids=true | all-gather | bytes 34816 | tf_op jit(solution)/shard_map/all_gather | solution.py:17
  145.2 26.9 %all-gather.10.cloned.1.call-done = f32[16,4,128,128]{3,2,1,0:T(8,128)} async-done(((f32[1,4,128,128]{3,2,1,0:T(8,128)}), f32[16,4,128,128]{3,2,1,0:T(8,128)}) %all-gather.10.cloned.1.call-update) | async-done | bytes 4194320 | tf_op jit(solution)/shard_map/all_gather | solution.py:17
  172.2 16.5 %while.25 = (s32[]{:T(128)}, f32[1,4,128,128]{3,2,1,0:T(8,128)S(1)}, s32[]{:T(128)}, f32[16,1,4,128]{3,2,1,0:T(4,128)S(1)}, f32[16,1,4,128,128]{4,3,2,1,0:T(8,128)}, /*index=5*/s32[]{:T(128)}, s32[]{:T(128)}, s32[]{:T(128)}) while((s32[]{:T(128)}, f32[1,4,128,128]{3,2,1,0:T(8,128)S(1)}, s32[]{:T(128)}, f32[16,1,4,128]{3,2,1,0:T(4,128)S(1)}, ...), condition=%wide.region_7.8_spmd, body=%wide.region_6.7_spmd.sunk | while | flops 131077 | bytes 792711 | solution.py:25
  188.7 2.8 %multiply_reduce_fusion.1 = (f32[4,512]{1,0:T(4,128)S(1)}, f32[4,512,128]{1,2,0:T(8,128)S(1)}) fusion(f32[4,512,128]{1,2,0:T(8,128)} %copy.46, f32[1,4,128,128]{3,2,1,0:T(8,128)S(1)} %get-tuple-element.94, f32[1,512,4,128]{3,1,2,0:T(8,128)S(1)} %bitcast.229, f32[1,4,128,512]{2,3,1,0:T(8,128)} %copy-done.5), kind=kOutput, calls=%fused_computation.80 | convolution fusion | flops 403699712 | bytes 4464640 | tf_op jit(solution)/shard_map/shtk,shkv->shtv/dot_general | solution.py:135
  194.3 23.4 %all-gather.8.cloned.1.call-done = bf16[1,512,1024]{1,2,0:T(8,128)(2,1)} async-done(((bf16[1,512,512]{1,2,0:T(8,128)(2,1)}), bf16[1,512,1024]{1,2,0:T(8,128)(2,1)}) %all-gather.8.cloned.1.call-update) | async-done | bytes 1048592 | tf_op jit(solution)/shard_map/all_gather | solution.py:182
  217.7 3.8 %multiply_reduce_fusion = (f32[512]{0:T(512)S(1)}, f32[512,1024]{1,0:T(8,128)}) fusion(bf16[1024,1024]{1,0:T(8,128)(2,1)S(1)} %copy-done, bf16[1,512,1024]{1,2,0:T(8,128)(2,1)} %all-gather.8.cloned.1.call-done), kind=kOutput, calls=%fused_computation.51 | convolution fusion | flops 1074789888 | bytes 5244928 | tf_op jit(solution)/shard_map/stc,cd->std/dot_general | solution.py:180
  221.5 4.9 %psum.7 = f32[1,512,1]{1,2,0:T(1,128)S(1)} all-reduce(f32[1,512,1]{1,2,0:T(1,128)S(1)} %bitcast.245), channel_id=1, replica_groups=mesh['sp'=16,'tp'=2] {'tp'}, use_global_device_ids=true, to_apply=%region_10.11 | all-reduce | flops 512 | bytes 4096 | tf_op jit(solution)/shard_map/psum | solution.py:186
  226.4 2.8 %fusion.65 = bf16[1,512,1024]{2,1,0:T(8,128)(2,1)} fusion(f32[512,1024]{1,0:T(8,128)} %get-tuple-element.181, f32[1024]{0:T(1024)S(1)} %copy-done.8, f32[512]{0:T(512)S(1)} %bitcast.247), kind=kLoop, calls=%fused_computation.67 | loop fusion | flops 1572864 | bytes 3151872 | tf_op jit(solution)/shard_map/convert_element_type | solution.py:187
  (153 shorter events, 73.4 us)
Async XLA Ops:
  6.5 211.1 %copy-start = (bf16[1024,1024]{1,0:T(8,128)(2,1)S(1)}, bf16[1024,1024]{1,0:T(8,128)(2,1)}, u32[]{:S(2)}) copy-start(bf16[1024,1024]{1,0:T(8,128)(2,1)} %param.24) | copy-start | bytes 6291460
  6.5 38.4 %all-gather.6.cloned.1.call-start = ((), (), s32[]{:S(2)}) async-start(), calls=%async_computation | async-start | bytes 3145728 | tf_op jit(solution)/shard_map/all_gather | solution.py:157
  10.7 161.4 %all-gather.10.cloned.1.call-start = ((), (), s32[]{:S(2)}) async-start(), calls=%async_computation.2 | async-start | bytes 4456448 | tf_op jit(solution)/shard_map/all_gather | solution.py:17
  44.9 3.7 %copy-start.11 = (bf16[2048,512]{1,0:T(8,128)(2,1)S(1)}, bf16[2048,512]{1,0:T(8,128)(2,1)}, u32[]{:S(2)}) copy-start(bf16[2048,512]{1,0:T(8,128)(2,1)} %param.19) | copy-start | bytes 6291460
  44.9 3.7 %copy-start.14 = (bf16[1,512,2048]{2,1,0:T(8,128)(2,1)S(1)}, bf16[1,512,2048]{2,1,0:T(8,128)(2,1)}, u32[]{:S(2)}) copy-start(bf16[1,512,2048]{2,1,0:T(8,128)(2,1)} %all-gather.6.cloned.1.call-done) | copy-start | bytes 6291460
  48.6 1.6 copy-start.12
  50.2 1.6 copy-start.13
  53.2 1.7 copy-start.3
  54.7 1.6 copy-start.7
  54.7 1.6 copy-start.9
  56.2 5.6 %slice-start = ((bf16[1,512,2048]{1,2,0:T(8,128)(2,1)}), bf16[1,512,512]{1,2,0:T(8,128)(2,1)S(1)}, s32[]{:S(2)}) async-start(bf16[1,512,2048]{1,2,0:T(8,128)(2,1)} %copy-done.3), calls=%async_computation.3 | async-start | bytes 1048576 | tf_op jit(solution)/shard_map/slice | solution.py:173
  123.2 0.7 copy-start.1
  123.2 3.3 %copy-start.6 = (f32[1,4,128,512]{2,3,1,0:T(8,128)S(1)}, f32[1,4,128,512]{2,3,1,0:T(8,128)}, u32[]{:S(2)}) copy-start(f32[1,4,128,512]{2,3,1,0:T(8,128)} %get-tuple-element.174) | copy-start | bytes 3145732
  123.9 93.7 %all-gather.8.cloned.1.call-start = ((), (), s32[]{:S(2)}) async-start(), calls=%async_computation.1 | async-start | bytes 1572864 | tf_op jit(solution)/shard_map/all_gather | solution.py:182
  127.5 1.0 copy-start.5
  172.2 16.5 %copy-start.2 = (f32[8,1,4,64,128]{4,3,0,2,1:T(8,128)S(1)}, f32[8,1,4,64,128]{4,3,0,2,1:T(8,128)}, u32[]{:S(2)}) copy-start(f32[8,1,4,64,128]{4,3,0,2,1:T(8,128)} %get-tuple-element.316) | copy-start | bytes 3145732
  188.7 2.9 %copy-start.10 = (f32[128]{0:T(128)S(1)}, f32[128]{0:T(128)}, u32[]{:S(2)}) copy-start(f32[128]{0:T(128)} %param.23) | copy-start | bytes 1540
  191.5 1.6 copy-start.4
  194.3 32.1 %copy-start.8 = (f32[1024]{0:T(1024)S(1)}, f32[1024]{0:T(1024)}, u32[]{:S(2)}) copy-start(f32[1024]{0:T(1024)} %param.25) | copy-start | bytes 12292
Sparse Core Ops, SparseCore 0:
  10.9 34.0 all-gather.5
  124.0 48.0 all-gather.9
  194.4 23.2 all-gather.7
where the time goes:
time: 239 us; the launch traced here: 236 us
  waiting for transfers between devices  84.5 us (35%)
  matrix products  62.7 us (26%)
  other arithmetic  33.2 us (14%)
  blocking collectives  21.7 us (9%)
  local copies, waits for them, and re-layouts  19.3 us (8%)
  between operations  13.3 us (6%)
    all_gather x1, waiting for transfers between devices, shards(): portion = lax.all_gather(normed, 'tp', axis=1, tiled=True)  34.1 us
    all_gather x1, waiting for transfers between devices, entering(): gathered = jax.tree.map(lambda a: lax.all_gather(a, axis), part)  26.9 us
    all_gather x1, waiting for transfers between devices, shards(): lax.all_gather(gated_out, 'tp', axis=2, tiled=True)  23.4 us
    all_gather x1, blocking collectives, entering(): gathered = jax.tree.map(lambda a: lax.all_gather(a, axis), part)  16.8 us
    add x14, other arithmetic, join_states(): jnp.exp(later_decay)[..., None] * earlier_state + later_state  15.7 us
    dot_general x8, matrix products, advance(): jnp.einsum('shtk,shkv->shtv', lifted_q, carried, precision=precise)  15.5 us
    dot_general x8, matrix products, advance(): jnp.einsum('shuk,shuv->shkv', weight_blk * jnp.exp(ending - running), val...  13 us
    dot_general x8, matrix products, advance(): jnp.einsum('shtk,shuk->shtu', lifted_q, lifted_k, precision=precise)  10.6 us
  transfers between devices with their start and end apart: 3, of which 3 were waited for; matrix products, arithmetic and copies ran while one was open for 1% of the time, Pallas kernels for 0%

commit v1 on v0

v1 whole, which is shorter than its diff:
```python
import functools

import jax
import jax.numpy as jnp
from jax import lax
from jax.experimental import pallas as pl
from jax.experimental.pallas import tpu as pltpu
from jax.sharding import PartitionSpec as P

KEY = 128
EPS = 1e-06
MESH = pl.DeviceIdType.MESH
F32 = jnp.float32
BF16 = jnp.bfloat16


def dot(a, b, dims=((1,), (0,))):
    return lax.dot_general(a, b, (dims, ((), ())), preferred_element_type=F32)


def kernel(
    cfg,
    tokens, gain, wq, wf, wi, wg, slack, sudden, head_gain, wo, out_gain,
    out,
    raw, w, ow, states, inner, lifted, gates, mids, cums, gated, proj,
    mine, theirs, tx, rx, inc_s, inc_d, exc_s, exc_d, ex_tx, ex_rx, entry,
    squares,
    w_sem, own_sem, raw_send, raw_recv, pair_send, pair_recv, ks_send, ks_recv,
    ex_send, ex_recv, g_send, g_recv, s_send, s_recv,
):
    n_sp, n_tp, seg, block, heads, model = cfg
    rows_all = seg * n_tp
    blocks = rows_all // block
    per_seg = seg // block
    hk = heads * KEY
    half = hk // 2
    chips = n_sp // 2
    steps = []
    d = 1
    while d < chips:
        steps.append(d)
        d *= 2
    p = lax.axis_index("sp")
    t = lax.axis_index("tp")
    core = lax.rem(p, 2)
    chip = p // 2
    partner = p + 1 - 2 * core

    for at, ref in enumerate((wq, wf, wi, wg)):
        pltpu.make_async_copy(ref, w.at[at], w_sem.at[at]).start()
    own_rows = pl.ds(pl.multiple_of(t * seg, seg), seg)
    own_copy = pltpu.make_async_copy(tokens, raw.at[own_rows], own_sem)
    own_copy.start()
    pltpu.make_async_copy(wo, ow, w_sem.at[4]).start()

    barrier = pltpu.get_barrier_semaphore()

    def greet(sp_at, tp_at):
        pl.semaphore_signal(barrier, inc=1, device_id=(sp_at, tp_at), device_id_type=MESH)

    for k in range(1, n_tp):
        greet(p, lax.rem(t + k, n_tp))
    greet(partner, t)
    for d in steps:
        @pl.when(chip + d < chips)
        def _():
            greet(p + 2 * d, t)

        @pl.when(chip >= d)
        def _():
            greet(p - 2 * d, t)
    peers = n_tp
    for d in steps:
        peers = peers + jnp.where(chip + d < chips, 1, 0) + jnp.where(chip >= d, 1, 0)
    pl.semaphore_wait(barrier, peers)

    def raw_copy(k, i, source):
        at = pl.ds(pl.multiple_of(source * seg + i * block, block), block)
        return pltpu.make_async_remote_copy(
            src_ref=tokens.at[pl.ds(i * block, block)],
            dst_ref=raw.at[at],
            send_sem=raw_send.at[k - 1, i],
            recv_sem=raw_recv.at[k - 1, i],
            device_id=(p, lax.rem(t + k, n_tp)),
            device_id_type=MESH,
        )

    for i in range(per_seg):
        for k in range(1, n_tp):
            raw_copy(k, i, t).start()

    row = lax.broadcasted_iota(jnp.int32, (block, block), 0)
    col = lax.broadcasted_iota(jnp.int32, (block, block), 1)
    causal = col <= row
    mid = block // 2 - 1
    sums = jnp.where(
        (col > mid) & (col <= row), 1.0, jnp.where((col <= mid) & (col > row), -1.0, 0.0)
    ).astype(BF16)

    def process(b):
        rows = pl.ds(pl.multiple_of(b * block, block), block)
        x = raw[rows, :].astype(F32)
        scale = lax.rsqrt(jnp.mean(x * x, axis=1, keepdims=True) + EPS)
        normed = (x * scale * gain[...]).astype(BF16)
        fr = dot(normed, w[1]).astype(BF16).astype(F32)
        values = dot(normed, w[2]).astype(BF16)
        weight = slack[...] / (1.0 + jnp.exp(fr))
        sd = sudden[rows, :]
        sd = jnp.concatenate(
            [jnp.broadcast_to(sd[:, h : h + 1], (block, KEY)) for h in range(heads)], axis=1
        )
        logs = jnp.log1p(-weight) + sd
        high = logs.astype(BF16)
        low = (logs - high.astype(F32)).astype(BF16)
        centred = dot(sums, high) + dot(sums, low)
        ending = centred[block - 1 : block, :]
        to_mid = logs[0:1, :] - centred[0:1, :]
        lifted_k = weight * jnp.exp(-centred)
        kept = (lifted_k * jnp.exp(ending)).astype(BF16)
        lifted_k = lifted_k.astype(BF16)
        mids[b] = jnp.broadcast_to(to_mid, (8, hk))
        cums[b] = jnp.broadcast_to(to_mid + ending, (8, hk))
        for h in range(heads):
            at = slice(h * KEY, (h + 1) * KEY)
            states[b, :, at] = dot(values[:, at], kept[:, at], ((0,), (0,)))
        qr = dot(normed, w[0]).astype(BF16).astype(F32) * KEY ** (-0.5)
        lifted_q = (qr * jnp.exp(centred)).astype(BF16)
        lifted[rows, :] = lifted_q
        gates[rows, :] = dot(normed, w[3]).astype(BF16)
        for h in range(heads):
            at = slice(h * KEY, (h + 1) * KEY)
            scores = dot(lifted_q[:, at], lifted_k[:, at], ((1,), (1,)))
            scores = jnp.where(causal, scores, 0.0).astype(BF16)
            inner[rows, at] = dot(scores, values[:, at])

    own_copy.wait()
    for at, ref in enumerate((wq, wf, wi, wg)):
        pltpu.make_async_copy(ref, w.at[at], w_sem.at[at]).wait()

    def own_block(i, carry):
        process(t * per_seg + i)
        return carry

    lax.fori_loop(0, per_seg, own_block, 0)
    for i in range(per_seg):
        for k in range(1, n_tp):
            source = lax.rem(t + n_tp - k, n_tp)
            raw_copy(k, i, source).wait_recv()
            process(source * per_seg + i)

    state = jnp.zeros((KEY, hk), F32)
    total = jnp.zeros((1, hk), F32)
    for b in range(blocks):
        fresh = states[b]
        step_log = cums[b][0:1, :]
        states[b] = state
        cums[b] = jnp.broadcast_to(total, (8, hk))
        state = jnp.exp(step_log) * state + fresh
        total = total + step_log
    decay = jnp.exp(total)

    def fill(ref, s, dec):
        width = dec.shape[1]
        ref[0:KEY, :] = s.astype(BF16)
        hi = dec.astype(BF16).astype(F32)
        lo = dec - hi
        at = lax.broadcasted_iota(jnp.int32, (16, width), 0)
        tail = jnp.where(at == 0, hi, jnp.where(at == 1, lo, 0.0))
        ref[KEY : KEY + 16, :] = tail.astype(BF16)

    def read(ref):
        s = ref[0:KEY, :].astype(F32)
        tail = ref[KEY : KEY + 16, :].astype(F32)
        return s, tail[0:1, :] + tail[1:2, :]

    fill(mine, state, decay)
    pair = pltpu.make_async_remote_copy(
        src_ref=mine, dst_ref=theirs, send_sem=pair_send, recv_sem=pair_recv,
        device_id=(partner, t), device_id_type=MESH,
    )
    pair.start()
    pair.wait_recv()
    their_s, their_d = read(theirs)
    first = core == 0
    joined_s = jnp.where(first, their_d * state + their_s, decay * their_s + state)
    joined_d = decay * their_d
    inc_s[...] = jnp.where(first, joined_s[:, :half], joined_s[:, half:])
    inc_d[...] = jnp.broadcast_to(
        jnp.where(first, joined_d[:, :half], joined_d[:, half:]), (8, half)
    )
    exc_s[...] = jnp.zeros_like(exc_s)
    exc_d[...] = jnp.ones_like(exc_d)

    def ks_copy(k, to):
        return pltpu.make_async_remote_copy(
            src_ref=tx.at[k], dst_ref=rx.at[k], send_sem=ks_send.at[k], recv_sem=ks_recv.at[k],
            device_id=(to, t), device_id_type=MESH,
        )

    for k, d in enumerate(steps):
        @pl.when(chip + d < chips)
        def _():
            fill(tx.at[k], inc_s[...], inc_d[0:1, :])
            ks_copy(k, p + 2 * d).start()

        @pl.when(chip >= d)
        def _():
            ks_copy(k, p).wait_recv()
            got_s, got_d = read(rx.at[k])
            exc_s[...] = exc_d[0:1, :] * got_s + exc_s[...]
            exc_d[...] = exc_d[...] * got_d
            if k < len(steps) - 1:
                inc_s[...] = inc_d[0:1, :] * got_s + inc_s[...]
                inc_d[...] = inc_d[...] * got_d

    ex_tx[...] = exc_s[...].astype(BF16)
    swap = pltpu.make_async_remote_copy(
        src_ref=ex_tx, dst_ref=ex_rx, send_sem=ex_send, recv_sem=ex_recv,
        device_id=(partner, t), device_id_type=MESH,
    )
    swap.start()
    swap.wait_recv()
    own_half = exc_s[...]
    other_half = ex_rx[...].astype(F32)
    both = jnp.concatenate(
        [jnp.where(first, own_half, other_half), jnp.where(first, other_half, own_half)], axis=1
    )
    their_s, their_d = read(theirs)
    entry[...] = jnp.where(first, both, their_d * both + their_s)

    def g_copy(k, b, source):
        rows = pl.ds(pl.multiple_of(b * block, block), block)
        return pltpu.make_async_remote_copy(
            src_ref=gated.at[t, rows],
            dst_ref=gated.at[source, rows],
            send_sem=g_send.at[k - 1, b],
            recv_sem=g_recv.at[k - 1, b],
            device_id=(p, lax.rem(t + k, n_tp)),
            device_id_type=MESH,
        )

    def finish(b, carry):
        rows = pl.ds(pl.multiple_of(b * block, block), block)
        at_start = jnp.exp(mids[b][0:1, :]) * (
            states[b] + jnp.exp(cums[b][0:1, :]) * entry[...]
        )
        at_start = at_start.astype(BF16)
        for h in range(heads):
            at = slice(h * KEY, (h + 1) * KEY)
            whole = inner[rows, at] + dot(lifted[rows, at], at_start[:, at], ((1,), (1,)))
            scale = lax.rsqrt(jnp.mean(whole * whole, axis=1, keepdims=True) + EPS)
            g = gates[rows, at].astype(F32)
            result = whole * scale * head_gain[...] * (g / (1.0 + jnp.exp(-g)))
            gated[t, rows, at] = result.astype(BF16)
        for k in range(1, n_tp):
            g_copy(k, b, t).start()
        return carry

    lax.fori_loop(0, blocks, finish, 0)

    def s_copy(k, b, source):
        return pltpu.make_async_remote_copy(
            src_ref=squares.at[t, b],
            dst_ref=squares.at[source, b],
            send_sem=s_send.at[k - 1, b],
            recv_sem=s_recv.at[k - 1, b],
            device_id=(p, lax.rem(t + k, n_tp)),
            device_id_type=MESH,
        )

    pltpu.make_async_copy(wo, ow, w_sem.at[4]).wait()

    def project(b, carry):
        rows = pl.ds(pl.multiple_of(b * block, block), block)
        for k in range(1, n_tp):
            g_copy(k, b, lax.rem(t + n_tp - k, n_tp)).wait_recv()
        acc = dot(gated[0, rows, :], ow[0:hk, :])
        for j in range(1, n_tp):
            acc = acc + dot(gated[j, rows, :], ow[j * hk : (j + 1) * hk, :])
        proj[rows, :] = acc
        line = jnp.sum(acc * acc, axis=1, keepdims=True)
        square = jnp.transpose(jnp.broadcast_to(line, (block, 128)))
        squares[t, b] = square[0:8, :]
        for k in range(1, n_tp):
            s_copy(k, b, t).start()
        return carry

    lax.fori_loop(0, blocks, project, 0)

    def close(b, carry):
        rows = pl.ds(pl.multiple_of(b * block, block), block)
        for k in range(1, n_tp):
            s_copy(k, b, lax.rem(t + n_tp - k, n_tp)).wait_recv()
        line = squares[0, b][0:1, :]
        for j in range(1, n_tp):
            line = line + squares[j, b][0:1, :]
        column = jnp.transpose(jnp.broadcast_to(line, (128, block)))[:, 0:1]
        out[rows, :] = (
            proj[rows, :] * lax.rsqrt(column * (1.0 / model) + EPS) * out_gain[...]
        ).astype(BF16)
        return carry

    lax.fori_loop(0, blocks, close, 0)

    for i in range(per_seg):
        for k in range(1, n_tp):
            raw_copy(k, i, t).wait_send()
    pair.wait_send()
    for k, d in enumerate(steps):
        @pl.when(chip + d < chips)
        def _():
            ks_copy(k, p + 2 * d).wait_send()
    swap.wait_send()
    for b in range(blocks):
        for k in range(1, n_tp):
            g_copy(k, b, t).wait_send()
            s_copy(k, b, t).wait_send()


def solution(mesh):
    n_sp, n_tp = mesh.shape["sp"], mesh.shape["tp"]

    def shards(tokens, gain, wq, wf, wi, wg, slack, sudden, head_gain, wo, out_gain):
        seg, model = tokens.shape[1:]
        hk = wq.shape[1]
        heads = hk // KEY
        features = wo.shape[1]
        rows_all = seg * n_tp
        block = min(128, seg)
        blocks = rows_all // block
        per_seg = seg // block
        half = hk // 2
        chips = n_sp // 2
        steps = max(1, (chips - 1).bit_length())
        peers = n_tp - 1
        any_spec = pl.BlockSpec(memory_space=pl.ANY)
        vmem = pl.BlockSpec(memory_space=pltpu.VMEM)
        dma = pltpu.SemaphoreType.DMA
        cfg = (n_sp, n_tp, seg, block, heads, model)
        call = pl.pallas_call(
            functools.partial(kernel, cfg),
            out_shape=jax.ShapeDtypeStruct((rows_all, features), BF16),
            in_specs=[
                any_spec, vmem, any_spec, any_spec, any_spec, any_spec,
                vmem, vmem, vmem, any_spec, vmem,
            ],
            out_specs=vmem,
            scratch_shapes=[
                pltpu.VMEM((rows_all, model), BF16),
                pltpu.VMEM((4, model, hk), BF16),
                pltpu.VMEM((hk * n_tp, features), BF16),
                pltpu.VMEM((blocks, KEY, hk), F32),
                pltpu.VMEM((rows_all, hk), F32),
                pltpu.VMEM((rows_all, hk), BF16),
                pltpu.VMEM((rows_all, hk), BF16),
                pltpu.VMEM((blocks, 8, hk), F32),
                pltpu.VMEM((blocks, 8, hk), F32),
                pltpu.VMEM((n_tp, rows_all, hk), BF16),
                pltpu.VMEM((rows_all, features), F32),
                pltpu.VMEM((KEY + 16, hk), BF16),
                pltpu.VMEM((KEY + 16, hk), BF16),
                pltpu.VMEM((steps, KEY + 16, half), BF16),
                pltpu.VMEM((steps, KEY + 16, half), BF16),
                pltpu.VMEM((KEY, half), F32),
                pltpu.VMEM((8, half), F32),
                pltpu.VMEM((KEY, half), F32),
                pltpu.VMEM((8, half), F32),
                pltpu.VMEM((KEY, half), BF16),
                pltpu.VMEM((KEY, half), BF16),
                pltpu.VMEM((KEY, hk), F32),
                pltpu.VMEM((n_tp, blocks, 8, 128), F32),
                dma((5,)), dma,
                dma((peers, per_seg)), dma((peers, per_seg)),
                dma, dma,
                dma((steps,)), dma((steps,)),
                dma, dma,
                dma((peers, blocks)), dma((peers, blocks)),
                dma((peers, blocks)), dma((peers, blocks)),
            ],
            compiler_params=pltpu.CompilerParams(
                collective_id=0, has_side_effects=True, vmem_limit_bytes=60 * 2**20
            ),
        )
        result = call(
            tokens[0], gain[None], wq, wf, wi, wg, slack[None], sudden[0],
            head_gain[None], wo, out_gain[None],
        )
        return result[None]

    placed = (
        P(None, ("sp", "tp"), None),
        P(),
        P(None, "tp"),
        P(None, "tp"),
        P(None, "tp"),
        P(None, "tp"),
        P("tp"),
        P(None, "sp", "tp"),
        P(),
        P(None, "tp"),
        P("tp"),
    )
    return jax.shard_map(
        shards, mesh=mesh, in_specs=placed, out_specs=P(None, "sp", "tp"), check_vma=False
    )
```

time: 239 us -> 63.3 us (0.26); the launches traced: 236 us -> 62.7 us
  waiting for transfers between devices: 84.5 us -> 0 us
  matrix products: 62.7 us -> 0 us
  Pallas kernels: 0 us -> 58.9 us
  other arithmetic: 33.2 us -> 0 us
  blocking collectives: 21.7 us -> 0 us
  local copies, waits for them, and re-layouts: 19.3 us -> 3.81 us
  between operations: 13.3 us -> 0.01 us
    all_gather x3 -> x0, waiting for transfers between devices: 84.4 us -> none  [the longest x1 34.1 us: shards(): portion = lax.all_gather(normed, 'tp', axis=1, tiled=True)]
    dot_general x38 -> x0, matrix products: 62.7 us -> none  [the longest x8 15.5 us: advance(): jnp.einsum('shtk,shkv->shtv', lifted_q, carried, precision=precise)]
    pallas_call x0 -> x1, Pallas kernels: none -> 58.9 us  [shards(): call(tokens[0], gain[None], wq, wf, wi, wg, slack[None], sudden[0], head_...]
    add x16 -> x0, other arithmetic: 21.3 us -> none  [the longest x14 15.7 us: join_states(): jnp.exp(later_decay)[..., None] * earlier_state + later_state]
    all_gather x1 -> x0, blocking collectives: 16.8 us -> none  [entering(): gathered = jax.tree.map(lambda a: lax.all_gather(a, axis), part)]
    squeeze x8 -> x0, local copies, waits for them, and re-layouts: 7.37 us -> none  [block_pass(): lax.scan(advance, initial, (by_block(query_rows), by_block(incoming_weigh...]
    convert_element_type x3 -> x0, other arithmetic: 6.43 us -> none  [the longest x1 2.8 us: shards(): (projected * lax.rsqrt(squares / D + epsilon) * output_norm_gain).astype(...]
    psum x1 -> x0, blocking collectives: 4.91 us -> none  [shards(): lax.psum(jnp.sum(projected * projected, axis=2, keepdims=True), 'tp')]
  transfers between devices with their start and end apart: 3 -> 0, of which waited for: 3 -> 0; matrix products, arithmetic and copies ran while one was open for 1% -> 0% of each run, Pallas kernels for 0% -> 0%
where the time goes in v1:
time: 63.3 us; the launch traced here: 62.7 us
  Pallas kernels  58.9 us (93%)
  local copies, waits for them, and re-layouts  3.81 us (6%)
    pallas_call x1, Pallas kernels, shards(): call(tokens[0], gain[None], wq, wf, wi, wg, slack[None], sudden[0], head_...  58.9 us
    unnamed x2, local copies, waits for them, and re-layouts  3.81 us

profile of v1, /device:TPU:28, one launch (start us, length us, event | category | flops | bytes accessed | tf_op | source)
XLA Modules:
  0.0 62.7 jit_solution(11909407012162532790)
XLA Ops:
  0.0 1.5 %copy.12 = f32[1,512,4]{2,1,0:T(8,128)} copy(f32[1,512,4]{1,2,0:T(4,128)} %param.18) | data formatting | bytes 16384 | tf_op args[7]
  1.6 58.9 %shard_map.109 = bf16[512,1024]{1,0:T(8,128)(2,1)} custom-call(bf16[256,2048]{1,0:T(8,128)(2,1)} %bitcast.8, f32[1,2048]{1,0:T(1,128)} %bitcast.10, bf16[2048,512]{1,0:T(8,128)(2,1)} %wq.1, bf16[2048,512]{1,0:T(8,128)(2,1)} %wf.1, bf16[2048,512]{1,0:T(8,128)(2,1)} %wi.1, bf16[2048,512]{1,0:T(8,128)(2,1)} %wg.1, f32[1,512]{1,0:T(1,128)} %bitcast.12, ...), custom_call_target="tpu_custom_call" | custom-call | tf_op jit(solution)/shard_map/pallas_call | solution.py:384
  60.4 2.3 %copy.14 = bf16[1,512,1024]{2,1,0:T(8,128)(2,1)} copy(bf16[1,512,1024]{2,1,0:T(8,128)(2,1)} %bitcast.7) | data formatting | bytes 2097152

commit v2 on v1

--- a/solution.py
+++ b/solution.py
@@ -22,7 +22,7 @@
     cfg,
     tokens, gain, wq, wf, wi, wg, slack, sudden, head_gain, wo, out_gain,
     out,
-    raw, w, ow, states, inner, lifted, gates, mids, cums, gated, proj,
+    raw, w, ow, states, inner, lifted, gates, mids, cums, gated, proj, centres, keys, vals, normal,
     mine, theirs, tx, rx, inc_s, inc_d, exc_s, exc_d, ex_tx, ex_rx, entry,
     squares,
     w_sem, own_sem, raw_send, raw_recv, pair_send, pair_recv, ks_send, ks_recv,
@@ -97,7 +97,7 @@
         (col > mid) & (col <= row), 1.0, jnp.where((col <= mid) & (col > row), -1.0, 0.0)
     ).astype(BF16)
 
-    def process(b):
+    def enter(b):
         rows = pl.ds(pl.multiple_of(b * block, block), block)
         x = raw[rows, :].astype(F32)
         scale = lax.rsqrt(jnp.mean(x * x, axis=1, keepdims=True) + EPS)
@@ -105,9 +105,13 @@
         fr = dot(normed, w[1]).astype(BF16).astype(F32)
         values = dot(normed, w[2]).astype(BF16)
         weight = slack[...] / (1.0 + jnp.exp(fr))
-        sd = sudden[rows, :]
+        sd = sudden[:, rows]
         sd = jnp.concatenate(
-            [jnp.broadcast_to(sd[:, h : h + 1], (block, KEY)) for h in range(heads)], axis=1
+            [
+                jnp.transpose(jnp.broadcast_to(sd[h : h + 1, :], (KEY, block)))
+                for h in range(heads)
+            ],
+            axis=1,
         )
         logs = jnp.log1p(-weight) + sd
         high = logs.astype(BF16)
@@ -123,6 +127,17 @@
         for h in range(heads):
             at = slice(h * KEY, (h + 1) * KEY)
             states[b, :, at] = dot(values[:, at], kept[:, at], ((0,), (0,)))
+        centres[rows, :] = centred
+        keys[rows, :] = lifted_k
+        vals[rows, :] = values
+        normal[rows, :] = normed
+
+    def leave(b):
+        rows = pl.ds(pl.multiple_of(b * block, block), block)
+        normed = normal[rows, :]
+        centred = centres[rows, :]
+        lifted_k = keys[rows, :]
+        values = vals[rows, :]
         qr = dot(normed, w[0]).astype(BF16).astype(F32) * KEY ** (-0.5)
         lifted_q = (qr * jnp.exp(centred)).astype(BF16)
         lifted[rows, :] = lifted_q
@@ -138,7 +153,8 @@
         pltpu.make_async_copy(ref, w.at[at], w_sem.at[at]).wait()
 
     def own_block(i, carry):
-        process(t * per_seg + i)
+        enter(t * per_seg + i)
+        leave(t * per_seg + i)
         return carry
 
     lax.fori_loop(0, per_seg, own_block, 0)
@@ -146,7 +162,9 @@
         for k in range(1, n_tp):
             source = lax.rem(t + n_tp - k, n_tp)
             raw_copy(k, i, source).wait_recv()
-            process(source * per_seg + i)
+            enter(source * per_seg + i)
+            if (i, k) != (per_seg - 1, n_tp - 1):
+                leave(source * per_seg + i)
 
     state = jnp.zeros((KEY, hk), F32)
     total = jnp.zeros((1, hk), F32)
@@ -179,6 +197,7 @@
         device_id=(partner, t), device_id_type=MESH,
     )
     pair.start()
+    leave(lax.rem(t + 1, n_tp) * per_seg + per_seg - 1)
     pair.wait_recv()
     their_s, their_d = read(theirs)
     first = core == 0
@@ -270,13 +289,23 @@
 
     pltpu.make_async_copy(wo, ow, w_sem.at[4]).wait()
 
+    def project_own(b, carry):
+        rows = pl.ds(pl.multiple_of(b * block, block), block)
+        depth = pl.ds(pl.multiple_of(t * hk, hk), hk)
+        proj[rows, :] = dot(gated[t, rows, :], ow[depth, :])
+        return carry
+
+    lax.fori_loop(0, blocks, project_own, 0)
+
     def project(b, carry):
         rows = pl.ds(pl.multiple_of(b * block, block), block)
         for k in range(1, n_tp):
             g_copy(k, b, lax.rem(t + n_tp - k, n_tp)).wait_recv()
-        acc = dot(gated[0, rows, :], ow[0:hk, :])
-        for j in range(1, n_tp):
-            acc = acc + dot(gated[j, rows, :], ow[j * hk : (j + 1) * hk, :])
+        acc = proj[rows, :]
+        for k in range(1, n_tp):
+            source = lax.rem(t + n_tp - k, n_tp)
+            depth = pl.ds(pl.multiple_of(source * hk, hk), hk)
+            acc = acc + dot(gated[source, rows, :], ow[depth, :])
         proj[rows, :] = acc
         line = jnp.sum(acc * acc, axis=1, keepdims=True)
         square = jnp.transpose(jnp.broadcast_to(line, (block, 128)))
@@ -333,13 +362,13 @@
         chips = n_sp // 2
         steps = max(1, (chips - 1).bit_length())
         peers = n_tp - 1
-        any_spec = pl.BlockSpec(memory_space=pl.ANY)
+        any_spec = pl.BlockSpec(memory_space=pltpu.HBM)
         vmem = pl.BlockSpec(memory_space=pltpu.VMEM)
         dma = pltpu.SemaphoreType.DMA
         cfg = (n_sp, n_tp, seg, block, heads, model)
         call = pl.pallas_call(
             functools.partial(kernel, cfg),
-            out_shape=jax.ShapeDtypeStruct((rows_all, features), BF16),
+            out_shape=pltpu.VMEM((rows_all, features), BF16),
             in_specs=[
                 any_spec, vmem, any_spec, any_spec, any_spec, any_spec,
                 vmem, vmem, vmem, any_spec, vmem,
@@ -357,6 +386,10 @@
                 pltpu.VMEM((blocks, 8, hk), F32),
                 pltpu.VMEM((n_tp, rows_all, hk), BF16),
                 pltpu.VMEM((rows_all, features), F32),
+                pltpu.VMEM((rows_all, hk), F32),
+                pltpu.VMEM((rows_all, hk), BF16),
+                pltpu.VMEM((rows_all, hk), BF16),
+                pltpu.VMEM((rows_all, model), BF16),
                 pltpu.VMEM((KEY + 16, hk), BF16),
                 pltpu.VMEM((KEY + 16, hk), BF16),
                 pltpu.VMEM((steps, KEY + 16, half), BF16),
@@ -378,11 +411,11 @@
                 dma((peers, blocks)), dma((peers, blocks)),
             ],
             compiler_params=pltpu.CompilerParams(
-                collective_id=0, has_side_effects=True, vmem_limit_bytes=60 * 2**20
+                collective_id=0, has_side_effects=True, vmem_limit_bytes=56 * 2**20
             ),
         )
         result = call(
-            tokens[0], gain[None], wq, wf, wi, wg, slack[None], sudden[0],
+            tokens[0], gain[None], wq, wf, wi, wg, slack[None], sudden[0].T,
             head_gain[None], wo, out_gain[None],
         )
         return result[None]

time: 63.3 us -> 57.9 us (0.915)
  local copies, waits for them, and re-layouts: 3.81 us -> 0.97 us
  Pallas kernels: 58.9 us -> 56.8 us
    unnamed x2 -> x1, local copies, waits for them, and re-layouts: 3.81 us -> 0.97 us
    pallas_call x1, Pallas kernels: 58.9 us -> 56.8 us  [shards(): call(tokens[0], gain[None], wq, wf, wi, wg, slack[None], sudden[0].T, hea...]
where the time goes in v2:
time: 57.9 us; the launch traced here: 57.7 us
  Pallas kernels  56.8 us (98%)
  local copies, waits for them, and re-layouts  0.97 us (2%)
    pallas_call x1, Pallas kernels, shards(): call(tokens[0], gain[None], wq, wf, wi, wg, slack[None], sudden[0].T, hea...  56.8 us

profile of v2, /device:TPU:28, one launch (start us, length us, event | category | flops | bytes accessed | tf_op | source)
XLA Modules:
  0.0 57.7 jit_solution(16808530923609866953)
XLA Ops:
  0.0 56.8 %shard_map.109 = bf16[512,1024]{1,0:T(8,128)(2,1)S(1)} custom-call(bf16[256,2048]{1,0:T(8,128)(2,1)} %bitcast.10, f32[1,2048]{1,0:T(1,128)} %bitcast.11, bf16[2048,512]{1,0:T(8,128)(2,1)} %wq.1, bf16[2048,512]{1,0:T(8,128)(2,1)} %wf.1, bf16[2048,512]{1,0:T(8,128)(2,1)} %wi.1, bf16[2048,512]{1,0:T(8,128)(2,1)} %wg.1, f32[1,512]{1,0:T(1,128)} %bitcast.14, ...), custom_call_target="tpu_custom_call" | custom-call | tf_op jit(solution)/shard_map/pallas_call | solution.py:417
  56.8 1.0 %copy.13 = bf16[1,512,1024]{2,1,0:T(8,128)(2,1)} copy(bf16[1,512,1024]{2,1,0:T(8,128)(2,1)S(1)} %bitcast.9) | data formatting | bytes 2097152

commit v3 on v2

--- a/solution.py
+++ b/solution.py
@@ -25,7 +25,7 @@
     raw, w, ow, states, inner, lifted, gates, mids, cums, gated, proj, centres, keys, vals, normal,
     mine, theirs, tx, rx, inc_s, inc_d, exc_s, exc_d, ex_tx, ex_rx, entry,
     squares,
-    w_sem, own_sem, raw_send, raw_recv, pair_send, pair_recv, ks_send, ks_recv,
+    w_sem, ow_sem, own_sem, raw_send, raw_recv, pair_send, pair_recv, ks_send, ks_recv,
     ex_send, ex_recv, g_send, g_recv, s_send, s_recv,
 ):
     n_sp, n_tp, seg, block, heads, model = cfg
@@ -51,7 +51,20 @@
     own_rows = pl.ds(pl.multiple_of(t * seg, seg), seg)
     own_copy = pltpu.make_async_copy(tokens, raw.at[own_rows], own_sem)
     own_copy.start()
-    pltpu.make_async_copy(wo, ow, w_sem.at[4]).start()
+    groups = half // KEY
+
+    def ow_copies():
+        for j in range(n_tp):
+            for h in range(heads):
+                place = j * heads + (h % groups) * 2 + h // groups
+                yield pltpu.make_async_copy(
+                    wo.at[pl.ds((j * heads + h) * KEY, KEY)],
+                    ow.at[pl.ds(place * KEY, KEY)],
+                    ow_sem.at[j * heads + h],
+                )
+
+    for copy in ow_copies():
+        copy.start()
 
     barrier = pltpu.get_barrier_semaphore()
 
@@ -141,7 +154,9 @@
         qr = dot(normed, w[0]).astype(BF16).astype(F32) * KEY ** (-0.5)
         lifted_q = (qr * jnp.exp(centred)).astype(BF16)
         lifted[rows, :] = lifted_q
-        gates[rows, :] = dot(normed, w[3]).astype(BF16)
+        g = dot(normed, w[3]).astype(BF16).astype(F32)
+        wide_gain = jnp.concatenate([head_gain[...]] * heads, axis=1)
+        gates[rows, :] = wide_gain * (g / (1.0 + jnp.exp(-g)))
         for h in range(heads):
             at = slice(h * KEY, (h + 1) * KEY)
             scores = dot(lifted_q[:, at], lifted_k[:, at], ((1,), (1,)))
@@ -203,79 +218,105 @@
     first = core == 0
     joined_s = jnp.where(first, their_d * state + their_s, decay * their_s + state)
     joined_d = decay * their_d
-    inc_s[...] = jnp.where(first, joined_s[:, :half], joined_s[:, half:])
-    inc_d[...] = jnp.broadcast_to(
-        jnp.where(first, joined_d[:, :half], joined_d[:, half:]), (8, half)
-    )
+    for g in range(groups):
+        near = slice(g * KEY, (g + 1) * KEY)
+        far = slice(half + g * KEY, half + (g + 1) * KEY)
+        inc_s[g] = jnp.where(first, joined_s[:, near], joined_s[:, far])
+        inc_d[g] = jnp.broadcast_to(
+            jnp.where(first, joined_d[:, near], joined_d[:, far]), (8, KEY)
+        )
     exc_s[...] = jnp.zeros_like(exc_s)
     exc_d[...] = jnp.ones_like(exc_d)
 
-    def ks_copy(k, to):
+    def ks_copy(k, g, to):
         return pltpu.make_async_remote_copy(
-            src_ref=tx.at[k], dst_ref=rx.at[k], send_sem=ks_send.at[k], recv_sem=ks_recv.at[k],
+            src_ref=tx.at[k, g], dst_ref=rx.at[k, g],
+            send_sem=ks_send.at[k, g], recv_sem=ks_recv.at[k, g],
             device_id=(to, t), device_id_type=MESH,
         )
 
-    for k, d in enumerate(steps):
-        @pl.when(chip + d < chips)
+    def ks_start(k, g):
+        @pl.when(chip + steps[k] < chips)
         def _():
-            fill(tx.at[k], inc_s[...], inc_d[0:1, :])
-            ks_copy(k, p + 2 * d).start()
-
-        @pl.when(chip >= d)
+            fill(tx.at[k, g], inc_s[g], inc_d[g][0:1, :])
+            ks_copy(k, g, p + 2 * steps[k]).start()
+
+    def ks_take(k, g):
+        @pl.when(chip >= steps[k])
         def _():
-            ks_copy(k, p).wait_recv()
-            got_s, got_d = read(rx.at[k])
-            exc_s[...] = exc_d[0:1, :] * got_s + exc_s[...]
-            exc_d[...] = exc_d[...] * got_d
+            ks_copy(k, g, p).wait_recv()
+            got_s, got_d = read(rx.at[k, g])
+            exc_s[g] = exc_d[g][0:1, :] * got_s + exc_s[g]
+            exc_d[g] = exc_d[g] * got_d
             if k < len(steps) - 1:
-                inc_s[...] = inc_d[0:1, :] * got_s + inc_s[...]
-                inc_d[...] = inc_d[...] * got_d
-
-    ex_tx[...] = exc_s[...].astype(BF16)
-    swap = pltpu.make_async_remote_copy(
-        src_ref=ex_tx, dst_ref=ex_rx, send_sem=ex_send, recv_sem=ex_recv,
-        device_id=(partner, t), device_id_type=MESH,
-    )
-    swap.start()
-    swap.wait_recv()
-    own_half = exc_s[...]
-    other_half = ex_rx[...].astype(F32)
-    both = jnp.concatenate(
-        [jnp.where(first, own_half, other_half), jnp.where(first, other_half, own_half)], axis=1
-    )
-    their_s, their_d = read(theirs)
-    entry[...] = jnp.where(first, both, their_d * both + their_s)
-
-    def g_copy(k, b, source):
-        rows = pl.ds(pl.multiple_of(b * block, block), block)
+                inc_s[g] = inc_d[g][0:1, :] * got_s + inc_s[g]
+                inc_d[g] = inc_d[g] * got_d
+
+    def swap_copy(g):
         return pltpu.make_async_remote_copy(
-            src_ref=gated.at[t, rows],
-            dst_ref=gated.at[source, rows],
-            send_sem=g_send.at[k - 1, b],
-            recv_sem=g_recv.at[k - 1, b],
+            src_ref=ex_tx.at[g], dst_ref=ex_rx.at[g],
+            send_sem=ex_send.at[g], recv_sem=ex_recv.at[g],
+            device_id=(partner, t), device_id_type=MESH,
+        )
+
+    def g_copy(k, g, b, source):
+        rows = pl.ds(pl.multiple_of(b * block, block), block)
+        return pltpu.make_async_remote_copy(
+            src_ref=gated.at[t, g, rows],
+            dst_ref=gated.at[source, g, rows],
+            send_sem=g_send.at[k - 1, g, b],
+            recv_sem=g_recv.at[k - 1, g, b],
             device_id=(p, lax.rem(t + k, n_tp)),
             device_id_type=MESH,
         )
 
-    def finish(b, carry):
-        rows = pl.ds(pl.multiple_of(b * block, block), block)
-        at_start = jnp.exp(mids[b][0:1, :]) * (
-            states[b] + jnp.exp(cums[b][0:1, :]) * entry[...]
-        )
-        at_start = at_start.astype(BF16)
-        for h in range(heads):
+    if steps:
+        for g in range(groups):
+            ks_start(0, g)
+    for k in range(len(steps) - 1):
+        for g in range(groups):
+            ks_take(k, g)
+            ks_start(k + 1, g)
+    for g in range(groups):
+        if steps:
+            ks_take(len(steps) - 1, g)
+        ex_tx[g] = exc_s[g].astype(BF16)
+        swap_copy(g).start()
+        swap_copy(g).wait_recv()
+        own_part = exc_s[g]
+        other_part = ex_rx[g].astype(F32)
+        pieces = (
+            jnp.where(first, own_part, other_part), jnp.where(first, other_part, own_part)
+        )
+        for c, piece in enumerate(pieces):
+            h = c * groups + g
             at = slice(h * KEY, (h + 1) * KEY)
-            whole = inner[rows, at] + dot(lifted[rows, at], at_start[:, at], ((1,), (1,)))
-            scale = lax.rsqrt(jnp.mean(whole * whole, axis=1, keepdims=True) + EPS)
-            g = gates[rows, at].astype(F32)
-            result = whole * scale * head_gain[...] * (g / (1.0 + jnp.exp(-g)))
-            gated[t, rows, at] = result.astype(BF16)
-        for k in range(1, n_tp):
-            g_copy(k, b, t).start()
-        return carry
-
-    lax.fori_loop(0, blocks, finish, 0)
+            past_s = theirs[0:KEY, at].astype(F32)
+            tail = theirs[KEY : KEY + 16, at].astype(F32)
+            past_d = tail[0:1, :] + tail[1:2, :]
+            entry[:, c * KEY : (c + 1) * KEY] = jnp.where(
+                first, piece, past_d * piece + past_s
+            )
+
+        def finish(b, carry):
+            rows = pl.ds(pl.multiple_of(b * block, block), block)
+            for c in range(2):
+                h = c * groups + g
+                at = slice(h * KEY, (h + 1) * KEY)
+                side = slice(c * KEY, (c + 1) * KEY)
+                at_start = jnp.exp(mids[b, 0:1, at]) * (
+                    states[b, :, at] + jnp.exp(cums[b, 0:1, at]) * entry[:, side]
+                )
+                whole = inner[rows, at] + dot(
+                    lifted[rows, at], at_start.astype(BF16), ((1,), (1,))
+                )
+                scale = lax.rsqrt(jnp.mean(whole * whole, axis=1, keepdims=True) + EPS)
+                gated[t, g, rows, side] = (whole * scale * gates[rows, at]).astype(BF16)
+            for k in range(1, n_tp):
+                g_copy(k, g, b, t).start()
+            return carry
+
+        lax.fori_loop(0, blocks, finish, 0)
 
     def s_copy(k, b, source):
         return pltpu.make_async_remote_copy(
@@ -287,25 +328,42 @@
             device_id_type=MESH,
         )
 
-    pltpu.make_async_copy(wo, ow, w_sem.at[4]).wait()
+    for copy in ow_copies():
+        copy.wait()
+
+    def depth_of(j, g):
+        return pl.ds(pl.multiple_of(j * hk + g * 2 * KEY, 2 * KEY), 2 * KEY)
 
     def project_own(b, carry):
         rows = pl.ds(pl.multiple_of(b * block, block), block)
-        depth = pl.ds(pl.multiple_of(t * hk, hk), hk)
-        proj[rows, :] = dot(gated[t, rows, :], ow[depth, :])
+        acc = dot(gated[t, 0, rows, :], ow[depth_of(t, 0), :])
+        for g in range(1, groups):
+            acc = acc + dot(gated[t, g, rows, :], ow[depth_of(t, g), :])
+        proj[rows, :] = acc
         return carry
 
     lax.fori_loop(0, blocks, project_own, 0)
 
+    def peers_part(b, g):
+        rows = pl.ds(pl.multiple_of(b * block, block), block)
+        acc = proj[rows, :]
+        for k in range(1, n_tp):
+            source = lax.rem(t + n_tp - k, n_tp)
+            g_copy(k, g, b, source).wait_recv()
+            acc = acc + dot(gated[source, g, rows, :], ow[depth_of(source, g), :])
+        return acc
+
+    for g in range(groups - 1):
+        def project_early(b, carry):
+            rows = pl.ds(pl.multiple_of(b * block, block), block)
+            proj[rows, :] = peers_part(b, g)
+            return carry
+
+        lax.fori_loop(0, blocks, project_early, 0)
+
     def project(b, carry):
         rows = pl.ds(pl.multiple_of(b * block, block), block)
-        for k in range(1, n_tp):
-            g_copy(k, b, lax.rem(t + n_tp - k, n_tp)).wait_recv()
-        acc = proj[rows, :]
-        for k in range(1, n_tp):
-            source = lax.rem(t + n_tp - k, n_tp)
-            depth = pl.ds(pl.multiple_of(source * hk, hk), hk)
-            acc = acc + dot(gated[source, rows, :], ow[depth, :])
+        acc = peers_part(b, groups - 1)
         proj[rows, :] = acc
         line = jnp.sum(acc * acc, axis=1, keepdims=True)
         square = jnp.transpose(jnp.broadcast_to(line, (block, 128)))
@@ -338,11 +396,14 @@
     for k, d in enumerate(steps):
         @pl.when(chip + d < chips)
         def _():
-            ks_copy(k, p + 2 * d).wait_send()
-    swap.wait_send()
+            for g in range(groups):
+                ks_copy(k, g, p + 2 * d).wait_send()
+    for g in range(groups):
+        swap_copy(g).wait_send()
     for b in range(blocks):
         for k in range(1, n_tp):
-            g_copy(k, b, t).wait_send()
+            for g in range(groups):
+                g_copy(k, g, b, t).wait_send()
             s_copy(k, b, t).wait_send()
 
 
@@ -358,7 +419,7 @@
         block = min(128, seg)
         blocks = rows_all // block
         per_seg = seg // block
-        half = hk // 2
+        groups = hk // 2 // KEY
         chips = n_sp // 2
         steps = max(1, (chips - 1).bit_length())
         peers = n_tp - 1
@@ -381,10 +442,10 @@
                 pltpu.VMEM((blocks, KEY, hk), F32),
                 pltpu.VMEM((rows_all, hk), F32),
                 pltpu.VMEM((rows_all, hk), BF16),
-                pltpu.VMEM((rows_all, hk), BF16),
+                pltpu.VMEM((rows_all, hk), F32),
                 pltpu.VMEM((blocks, 8, hk), F32),
                 pltpu.VMEM((blocks, 8, hk), F32),
-                pltpu.VMEM((n_tp, rows_all, hk), BF16),
+                pltpu.VMEM((n_tp, groups, rows_all, 2 * KEY), BF16),
                 pltpu.VMEM((rows_all, features), F32),
                 pltpu.VMEM((rows_all, hk), F32),
                 pltpu.VMEM((rows_all, hk), BF16),
@@ -392,22 +453,22 @@
                 pltpu.VMEM((rows_all, model), BF16),
                 pltpu.VMEM((KEY + 16, hk), BF16),
                 pltpu.VMEM((KEY + 16, hk), BF16),
-                pltpu.VMEM((steps, KEY + 16, half), BF16),
-                pltpu.VMEM((steps, KEY + 16, half), BF16),
-                pltpu.VMEM((KEY, half), F32),
-                pltpu.VMEM((8, half), F32),
-                pltpu.VMEM((KEY, half), F32),
-                pltpu.VMEM((8, half), F32),
-                pltpu.VMEM((KEY, half), BF16),
-                pltpu.VMEM((KEY, half), BF16),
-                pltpu.VMEM((KEY, hk), F32),
+                pltpu.VMEM((steps, groups, KEY + 16, KEY), BF16),
+                pltpu.VMEM((steps, groups, KEY + 16, KEY), BF16),
+                pltpu.VMEM((groups, KEY, KEY), F32),
+                pltpu.VMEM((groups, 8, KEY), F32),
+                pltpu.VMEM((groups, KEY, KEY), F32),
+                pltpu.VMEM((groups, 8, KEY), F32),
+                pltpu.VMEM((groups, KEY, KEY), BF16),
+                pltpu.VMEM((groups, KEY, KEY), BF16),
+                pltpu.VMEM((KEY, 2 * KEY), F32),
                 pltpu.VMEM((n_tp, blocks, 8, 128), F32),
-                dma((5,)), dma,
+                dma((4,)), dma((heads * n_tp,)), dma,
                 dma((peers, per_seg)), dma((peers, per_seg)),
                 dma, dma,
-                dma((steps,)), dma((steps,)),
-                dma, dma,
-                dma((peers, blocks)), dma((peers, blocks)),
+                dma((steps, groups)), dma((steps, groups)),
+                dma((groups,)), dma((groups,)),
+                dma((peers, groups, blocks)), dma((peers, groups, blocks)),
                 dma((peers, blocks)), dma((peers, blocks)),
             ],
             compiler_params=pltpu.CompilerParams(

time: 57.9 us -> 56.8 us (0.981)
  Pallas kernels: 56.8 us -> 55.6 us
    pallas_call x1, Pallas kernels: 56.8 us -> 55.6 us  [shards(): call(tokens[0], gain[None], wq, wf, wi, wg, slack[None], sudden[0].T, hea...]
where the time goes in v3:
time: 56.8 us; the launch traced here: 56.6 us
  Pallas kernels  55.6 us (98%)
  local copies, waits for them, and re-layouts  0.97 us (2%)
    pallas_call x1, Pallas kernels, shards(): call(tokens[0], gain[None], wq, wf, wi, wg, slack[None], sudden[0].T, hea...  55.6 us

profile of v3, /device:TPU:28, one launch (start us, length us, event | category | flops | bytes accessed | tf_op | source)
XLA Modules:
  0.0 56.6 jit_solution(4866600811789915147)
XLA Ops:
  0.0 55.6 %shard_map.109 = bf16[512,1024]{1,0:T(8,128)(2,1)S(1)} custom-call(bf16[256,2048]{1,0:T(8,128)(2,1)} %bitcast.10, f32[1,2048]{1,0:T(1,128)} %bitcast.11, bf16[2048,512]{1,0:T(8,128)(2,1)} %wq.1, bf16[2048,512]{1,0:T(8,128)(2,1)} %wf.1, bf16[2048,512]{1,0:T(8,128)(2,1)} %wi.1, bf16[2048,512]{1,0:T(8,128)(2,1)} %wg.1, f32[1,512]{1,0:T(1,128)} %bitcast.14, ...), custom_call_target="tpu_custom_call" | custom-call | tf_op jit(solution)/shard_map/pallas_call | solution.py:478
  55.6 1.0 %copy.13 = bf16[1,512,1024]{2,1,0:T(8,128)(2,1)} copy(bf16[1,512,1024]{2,1,0:T(8,128)(2,1)S(1)} %bitcast.9) | data formatting | bytes 2097152

commit v4 on v3

--- a/solution.py
+++ b/solution.py
@@ -212,7 +212,6 @@
         device_id=(partner, t), device_id_type=MESH,
     )
     pair.start()
-    leave(lax.rem(t + 1, n_tp) * per_seg + per_seg - 1)
     pair.wait_recv()
     their_s, their_d = read(theirs)
     first = core == 0
@@ -273,6 +272,7 @@
     if steps:
         for g in range(groups):
             ks_start(0, g)
+    leave(lax.rem(t + 1, n_tp) * per_seg + per_seg - 1)
     for k in range(len(steps) - 1):
         for g in range(groups):
             ks_take(k, g)

time: 56.8 us -> 57.4 us (1.011)
  no operation moved by 1% of the time
where the time goes in v4:
time: 57.4 us; the launch traced here: 56.9 us
  Pallas kernels  55.9 us (97%)
  local copies, waits for them, and re-layouts  0.97 us (2%)
    pallas_call x1, Pallas kernels, shards(): call(tokens[0], gain[None], wq, wf, wi, wg, slack[None], sudden[0].T, hea...  55.9 us

profile of v4, /device:TPU:28, one launch (start us, length us, event | category | flops | bytes accessed | tf_op | source)
XLA Modules:
  0.0 56.9 jit_solution(14113711165032005184)
XLA Ops:
  0.0 55.9 %shard_map.109 = bf16[512,1024]{1,0:T(8,128)(2,1)S(1)} custom-call(bf16[256,2048]{1,0:T(8,128)(2,1)} %bitcast.10, f32[1,2048]{1,0:T(1,128)} %bitcast.11, bf16[2048,512]{1,0:T(8,128)(2,1)} %wq.1, bf16[2048,512]{1,0:T(8,128)(2,1)} %wf.1, bf16[2048,512]{1,0:T(8,128)(2,1)} %wi.1, bf16[2048,512]{1,0:T(8,128)(2,1)} %wg.1, f32[1,512]{1,0:T(1,128)} %bitcast.14, ...), custom_call_target="tpu_custom_call" | custom-call | tf_op jit(solution)/shard_map/pallas_call | solution.py:478
  55.9 1.0 %copy.13 = bf16[1,512,1024]{2,1,0:T(8,128)(2,1)} copy(bf16[1,512,1024]{2,1,0:T(8,128)(2,1)S(1)} %bitcast.9) | data formatting | bytes 2097152
